TPU v7x, 32 devices: a whole 2x2x4 slice. The times are simulated.
32 devices in a mesh: sp: 16 (over z, y, x), tp: 2 (over core).
Axes of the slice: x: 2, y: 2, z: 4, core: 2. Of those that a mesh axis runs over, the one named last changes fastest.
Arguments:
- resid: bfloat16 [3072, 2048], P('sp'), may hold values from -6 to 6
- query: bfloat16 [3072, 2048], P('sp', 'tp'), may hold values from -6 to 6
- key: bfloat16 [3072, 1024], P('sp', 'tp'), may hold values from -6 to 6
- value: bfloat16 [3072, 1024], P('sp', 'tp'), may hold values from -6 to 6
- q_gain: float32 [128], replicated, may hold values from 0.3 to 5, as said below
- k_gain: float32 [128], replicated, may hold values from 0.3 to 5, as said below
- out_weight: bfloat16 [2048, 2048], P('tp'), may hold values from -0.125 to 0.125
- norm_gain: float32 [2048], replicated, may hold values from 0.1 to 1.9
- gate_weight: bfloat16 [2048, 5632], P('sp', 'tp'), may hold values from -0.125 to 0.125
- up_weight: bfloat16 [2048, 5632], P('sp', 'tp'), may hold values from -0.125 to 0.125
- down_weight: bfloat16 [5632, 2048], P('tp', 'sp'), may hold values from -0.078125 to 0.078125
Outputs:
- mixed: bfloat16 [3072, 2048], P(('sp', 'tp'))
Inputs may be any that keep to these rules, and one draw needn't show every extreme that they name: `q_gain`: positive gains. `k_gain`: positive gains.
All inputs are finite; a program needn't handle non-finite values.
Results may differ from a plain program's by a relative error of at most 0.012.
The roundings to bfloat16 on the way count: a program that leaves them out, or rounds other values in their place, can miss the bound.
Values may be sent and summed in bfloat16 or wider, within the bound.
A program may use at most 128 MiB of HBM per device.

v0:
```python
import jax
import jax.numpy as jnp
from jax import lax
from jax.sharding import PartitionSpec as P

GRID_W = 64
EPSILON = 1e-06


def rotate(values, positions):
    dim_size = values.shape[-1]
    half_dim = dim_size // 2
    quarter = half_dim // 2
    inverse = 10000.0 ** (-jnp.arange(quarter, dtype=jnp.float32) / quarter)
    outputs = []
    for axis_pos, coords in enumerate((positions // GRID_W, positions % GRID_W)):
        angles = coords.astype(jnp.float32)[:, None] * inverse[None, :]
        cosine = jnp.cos(angles)[:, None, :]
        sine = jnp.sin(angles)[:, None, :]
        section = values[..., axis_pos * half_dim : (axis_pos + 1) * half_dim]
        first_half = section[..., :quarter]
        second_half = section[..., quarter:]
        outputs += [
            first_half * cosine - second_half * sine,
            second_half * cosine + first_half * sine,
        ]
    return jnp.concatenate(outputs, axis=-1)


def prepare(projected, gain, positions):
    values = projected.astype(jnp.float32)
    normed = values * lax.rsqrt(jnp.mean(values * values, axis=-1, keepdims=True) + EPSILON) * gain
    return rotate(normed, positions).astype(jnp.bfloat16)


def normalize(stream, gain):
    values = stream.astype(jnp.float32)
    return (
        values * lax.rsqrt(jnp.mean(values * values, axis=-1, keepdims=True) + EPSILON) * gain
    ).astype(jnp.bfloat16)


def body(
    resid,
    query,
    key,
    value,
    q_gain,
    k_gain,
    out_weight,
    norm_gain,
    gate_weight,
    up_weight,
    down_weight,
):
    rows_here = query.shape[0]
    head_dim = q_gain.shape[0]
    heads_here = query.shape[1] // head_dim
    kv_here = key.shape[1] // head_dim
    group_size = heads_here // kv_here
    score_scale = head_dim ** (-0.5)
    positions = lax.axis_index("sp") * rows_here + jnp.arange(rows_here, dtype=jnp.int32)
    q_rot = prepare(query.reshape(rows_here, heads_here, head_dim), q_gain, positions)
    k_rot = prepare(key.reshape(rows_here, kv_here, head_dim), k_gain, positions)
    val_rows = value.reshape(rows_here, kv_here, head_dim)
    grouped = q_rot.reshape(rows_here, kv_here, group_size, head_dim)

    def key_block(carry, block):
        maxima, totals, accum = carry
        block_keys, block_vals = block
        scores = (
            jnp.einsum("qkgd,skd->kgqs", grouped, block_keys, preferred_element_type=jnp.float32)
            * score_scale
        )
        new_max = jnp.maximum(maxima, jnp.max(scores, axis=-1))
        shrink = jnp.exp(maxima - new_max)
        weights = jnp.exp(scores - new_max[..., None])
        totals = totals * shrink + jnp.sum(weights, axis=-1)
        accum = accum * shrink[..., None] + jnp.einsum(
            "kgqs,skd->kgqd",
            weights.astype(jnp.bfloat16),
            block_vals,
            preferred_element_type=jnp.float32,
        )
        return ((new_max, totals, accum), None)

    start_max = jnp.full((kv_here, group_size, rows_here), -1e30, jnp.float32)
    start_total = jnp.zeros((kv_here, group_size, rows_here), jnp.float32)
    start_accum = jnp.zeros((kv_here, group_size, rows_here, head_dim), jnp.float32)
    carry = (start_max, start_total, start_accum)
    key_part = lax.all_gather(k_rot, "sp", axis=0, tiled=True)
    val_part = lax.all_gather(val_rows, "sp", axis=0, tiled=True)
    length = key_part.shape[0]
    factor = 4
    span = rows_here * factor
    turns = length // span
    key_blocks = key_part.reshape(turns, span, kv_here, head_dim)
    val_blocks = val_part.reshape(turns, span, kv_here, head_dim)
    carry, _ = lax.scan(key_block, carry, (key_blocks, val_blocks))
    maxima, totals, accum = carry
    attn = (
        jnp.transpose(accum / totals[..., None], (2, 0, 1, 3))
        .reshape(rows_here, heads_here * head_dim)
        .astype(jnp.bfloat16)
    )
    share = rows_here // lax.axis_size("tp")
    my_first = lax.axis_index("tp") * share
    proj = lax.psum_scatter(
        jnp.dot(attn, out_weight, preferred_element_type=jnp.float32).astype(jnp.bfloat16),
        "tp",
        scatter_dimension=0,
        tiled=True,
    ).astype(jnp.float32)
    my_resid = lax.dynamic_slice_in_dim(resid, my_first, share, 0)
    my_stream = (my_resid.astype(jnp.float32) + proj).astype(jnp.bfloat16)
    mixer_rows = lax.all_gather(normalize(my_stream, norm_gain), "tp", axis=0, tiled=True)

    def add_rows(shard_rows):
        return jnp.dot(mixer_rows, shard_rows, preferred_element_type=jnp.float32)

    gate = add_rows(lax.all_gather(gate_weight, "sp", axis=0, tiled=True))
    up_part = add_rows(lax.all_gather(up_weight, "sp", axis=0, tiled=True))
    hidden = (jax.nn.silu(gate) * up_part).astype(jnp.bfloat16)
    down_whole = lax.all_gather(down_weight, "sp", axis=1, tiled=True)
    down = lax.psum_scatter(
        jnp.dot(hidden, down_whole, preferred_element_type=jnp.float32).astype(jnp.bfloat16),
        "tp",
        scatter_dimension=0,
        tiled=True,
    ).astype(jnp.float32)
    return (my_stream.astype(jnp.float32) + 0.5 * down).astype(jnp.bfloat16)


def solution(mesh):
    placed = (
        P("sp", None),
        P("sp", "tp"),
        P("sp", "tp"),
        P("sp", "tp"),
        P(),
        P(),
        P("tp", None),
        P(),
        P("sp", "tp"),
        P("sp", "tp"),
        P("tp", "sp"),
    )
    return jax.shard_map(
        body, mesh=mesh, in_specs=placed, out_specs=P(("sp", "tp"), None), check_vma=False
    )
```

profile of v0, /device:TPU:0, one launch (start us, length us, event | category | flops | bytes accessed | tf_op | source)
XLA Modules:
  0.0 702.4 jit_solution(25329568361684075)
XLA Ops:
  15.1 67.4 %all-gather.6.cloned.1.call-done = bf16[3072,4,128]{2,1,0:T(4,128)(2,1)} async-done(((bf16[192,4,128]{2,1,0:T(4,128)(2,1)}), bf16[3072,4,128]{2,1,0:T(4,128)(2,1)}) %all-gather.6.cloned.1.call-update) | async-done | bytes 3145744 | tf_op jit(solution)/shard_map/all_gather | solution.py:91
  82.5 69.2 %all-gather.8.cloned.1.call-done = bf16[3072,4,128]{2,1,0:T(4,128)(2,1)} async-done(((bf16[192,4,128]{2,1,0:T(4,128)(2,1)}), bf16[3072,4,128]{2,1,0:T(4,128)(2,1)}) %all-gather.8.cloned.1.call-update) | async-done | bytes 3145744 | tf_op jit(solution)/shard_map/all_gather | solution.py:92
  151.7 40.1 %while.15 = (s32[]{:T(128)}, f32[4,2,192]{2,1,0:T(2,128)S(1)}, f32[4,2,192]{2,1,0:T(2,128)S(1)}, f32[4,2,192,128]{3,2,1,0:T(8,128)S(1)}, bf16[4,768,4,128]{3,2,1...) while((s32[]{:T(128)}, f32[4,2,192]{2,1,0:T(2,128)S(1)}, ...), condition=%wide.region_5.6_spmd.clone, body=%wide.region_2.5_spmd.clone.sunk | while | flops 614014464 | bytes 39813256 | solution.py:99
  151.7 1.9 constant_dynamic-slice_fusion.3
  153.6 2.9 bitcast_reduce_fusion.2
  156.5 3.5 fusion.42
  161.7 1.9 constant_dynamic-slice_fusion.3
  163.6 2.9 bitcast_reduce_fusion.2
  166.6 3.5 fusion.42
  171.7 1.9 constant_dynamic-slice_fusion.3
  173.6 2.9 bitcast_reduce_fusion.2
  176.6 3.5 fusion.42
  181.7 1.9 constant_dynamic-slice_fusion.3
  183.7 2.9 bitcast_reduce_fusion.2
  186.6 3.5 fusion.42
  192.8 4.1 convolution_convert_fusion.1
  198.7 5.1 reduce-scatter.3.cloned.1.call-done
  205.2 2.5 all_gather.20
  207.7 141.2 %all-gather.10.cloned.1.call-done = bf16[2048,2816]{1,0:T(8,128)(2,1)} async-done(((bf16[128,2816]{1,0:T(8,128)(2,1)}), bf16[2048,2816]{1,0:T(8,128)(2,1)}) %all-gather.10.cloned.1.call-update) | async-done | bytes 11534352 | tf_op jit(solution)/shard_map/all_gather | solution.py:121
  348.9 6.7 fusion.24
  355.6 135.6 %all-gather.12.cloned.1.call-done = bf16[2048,2816]{1,0:T(8,128)(2,1)} async-done(((bf16[128,2816]{1,0:T(8,128)(2,1)}), bf16[2048,2816]{1,0:T(8,128)(2,1)}) %all-gather.12.cloned.1.call-update) | async-done | bytes 11534352 | tf_op jit(solution)/shard_map/all_gather | solution.py:122
  491.2 182.8 %all-gather.14.cloned.1.call-done = bf16[2816,2048]{1,0:T(8,128)(2,1)} async-done(((bf16[2816,128]{1,0:T(8,128)(2,1)}), bf16[2816,2048]{1,0:T(8,128)(2,1)}) %all-gather.14.cloned.1.call-update) | async-done | bytes 11534352 | tf_op jit(solution)/shard_map/all_gather | solution.py:124
  674.0 13.2 %convolution_convert_fusion = bf16[192,2048]{1,0:T(8,128)(2,1)} fusion(bf16[2816,2048]{1,0:T(8,128)(2,1)} %all-gather.14.cloned.1.call-done, bf16[192,2048]{1,0:T(8,128)(2,1)S(1)} %all_gather.20, bf16[2048,2816]{1,0:T(8,128)(2,1)} %all-gather.12.cloned.1.call-done, f32[192,2816]{1,0:T(8,128)S(1)} %fusion.24), kind=kOutput, calls=%fused_computation.23 | convolution fusion | flops 4432822272 | bytes 26804224 | tf_op jit(solution)/shard_map/dot_general | solution.py:126
  687.2 6.5 reduce-scatter.5.cloned.1.call-done
  (81 shorter events, 20.8 us)
Async XLA Ops:
  6.5 5.2 copy-start.2
  6.5 6.1 copy-start.1
  6.5 75.9 %all-gather.6.cloned.1.call-start = ((), (), s32[]{:S(2)}) async-start(), calls=%async_computation.2 | async-start | bytes 3342336 | tf_op jit(solution)/shard_map/all_gather | solution.py:91
  8.0 5.3 copy-start.5
  11.7 140.0 %all-gather.8.cloned.1.call-start = ((), (), s32[]{:S(2)}) async-start(), calls=%async_computation.3 | async-start | bytes 3342336 | tf_op jit(solution)/shard_map/all_gather | solution.py:92
  12.5 191.2 %reduce-scatter.3.cloned.1.call-start = ((), (), s32[]{:S(2)}) async-start(), calls=%async_computation.4 | async-start | bytes 1179648 | tf_op jit(solution)/shard_map/reduce_scatter | solution.py:108
  156.5 3.8 copy-start
  166.5 3.8 copy-start
  176.6 3.8 copy-start
  186.6 3.8 copy-start
  192.5 11.3 %copy-start.3 = (bf16[192,2048]{1,0:T(8,128)(2,1)S(1)}, bf16[192,2048]{1,0:T(8,128)(2,1)}, u32[]{:S(2)}) copy-start(bf16[192,2048]{1,0:T(8,128)(2,1)} %param.13) | copy-start | bytes 2359300
  192.7 12.3 %copy-start.4 = (f32[2048]{0:T(1024)S(1)}, f32[2048]{0:T(1024)}, u32[]{:S(2)}) copy-start(f32[2048]{0:T(1024)} %param.20) | copy-start | bytes 24580
  196.9 152.0 %all-gather.10.cloned.1.call-start = ((), (), s32[]{:S(2)}) async-start(), calls=%async_computation.5 | async-start | bytes 12255232 | tf_op jit(solution)/shard_map/all_gather | solution.py:121
  197.5 293.7 %all-gather.12.cloned.1.call-start = ((), (), s32[]{:S(2)}) async-start(), calls=%async_computation.6 | async-start | bytes 12255232 | tf_op jit(solution)/shard_map/all_gather | solution.py:122
  198.1 475.9 %all-gather.14.cloned.1.call-start = ((), (), s32[]{:S(2)}) async-start(), calls=%async_computation.7 | async-start | bytes 12255232 | tf_op jit(solution)/shard_map/all_gather | solution.py:124
  198.6 495.1 %reduce-scatter.5.cloned.1.call-start = ((), (), s32[]{:S(2)}) async-start(), calls=%async_computation.8 | async-start | bytes 1179648 | tf_op jit(solution)/shard_map/reduce_scatter | solution.py:125
Sparse Core Ops, SparseCore 0:
  11.9 70.5 all-gather.5
  85.2 66.3 all-gather.7
  197.0 6.6 reduce-scatter.2
  206.4 142.5 all-gather.9
  351.5 139.5 all-gather.11
  493.7 180.2 all-gather.13
  687.3 6.3 reduce-scatter.4
where the time goes:
time: 703 us; the launch traced here: 702 us
  waiting for transfers between devices  609 us (87%)
  matrix products  41.2 us (6%)
  other arithmetic  23.7 us (3%)
  between operations  13.8 us (2%)
  local copies, waits for them, and re-layouts  11.4 us (2%)
    all_gather x1, waiting for transfers between devices, body(): down_whole = lax.all_gather(down_weight, 'sp', axis=1, tiled=True)  183 us
    all_gather x1, waiting for transfers between devices, body(): gate = add_rows(lax.all_gather(gate_weight, 'sp', axis=0, tiled=True))  141 us
    all_gather x1, waiting for transfers between devices, body(): up_part = add_rows(lax.all_gather(up_weight, 'sp', axis=0, tiled=True))  136 us
    all_gather x1, waiting for transfers between devices, body(): val_part = lax.all_gather(val_rows, 'sp', axis=0, tiled=True)  69.2 us
    all_gather x1, waiting for transfers between devices, body(): key_part = lax.all_gather(k_rot, 'sp', axis=0, tiled=True)  67.4 us
    reduce_sum x4, other arithmetic, key_block(): totals = totals * shrink + jnp.sum(weights, axis=-1)  14.2 us
  transfers between devices with their start and end apart: 7, of which 7 were waited for; matrix products, arithmetic and copies ran while one was open for 2% of the time, Pallas kernels for 0%

commit v1 on v0

--- a/solution.py
+++ b/solution.py
@@ -88,7 +88,12 @@
     start_total = jnp.zeros((kv_here, group_size, rows_here), jnp.float32)
     start_accum = jnp.zeros((kv_here, group_size, rows_here, head_dim), jnp.float32)
     carry = (start_max, start_total, start_accum)
-    key_part = lax.all_gather(k_rot, "sp", axis=0, tiled=True)
+    ring = [k_rot]
+    for hop in range(15):
+        ring.append(lax.ppermute(ring[-1], "sp", [(dev, (dev + 1) % 16) for dev in range(16)]))
+    key_part = jnp.roll(
+        jnp.concatenate(ring[::-1], axis=0), (lax.axis_index("sp") + 1) * ring[0].shape[0], axis=0
+    )
     val_part = lax.all_gather(val_rows, "sp", axis=0, tiled=True)
     length = key_part.shape[0]
     factor = 4

time: 703 us -> 751 us (1.068)
  local copies, waits for them, and re-layouts: 11.4 us -> 35 us
  waiting for transfers between devices: 609 us -> 624 us
    ppermute x0 -> x15, waiting for transfers between devices: none -> 154 us  [body(): lax.ppermute(ring[-1], 'sp', [(dev, (dev + 1) % 16) for dev in range(16)])]
    all_gather x1, waiting for transfers between devices: 69.2 us -> 0.01 us  [body(): val_part = lax.all_gather(val_rows, 'sp', axis=0, tiled=True)]
    all_gather x1 -> x0, waiting for transfers between devices: 67.4 us -> none  [body(): key_part = lax.all_gather(k_rot, 'sp', axis=0, tiled=True)]
    unnamed x11 -> x68, local copies, waits for them, and re-layouts: 0.17 us -> 21.5 us
  transfers between devices with their start and end apart: 7 -> 21, of which waited for: 7 -> 20; matrix products, arithmetic and copies ran while one was open for 2% -> 5% of each run, Pallas kernels for 0% -> 0%
where the time goes in v1:
time: 751 us; the launch traced here: 750 us
  waiting for transfers between devices  624 us (83%)
  matrix products  48 us (6%)
  local copies, waits for them, and re-layouts  35 us (5%)
  other arithmetic  22.4 us (3%)
  between operations  13.9 us (2%)
    all_gather x1, waiting for transfers between devices, body(): down_whole = lax.all_gather(down_weight, 'sp', axis=1, tiled=True)  176 us
    ppermute x15, waiting for transfers between devices, body(): lax.ppermute(ring[-1], 'sp', [(dev, (dev + 1) % 16) for dev in range(16)])  154 us
    all_gather x1, waiting for transfers between devices, body(): up_part = add_rows(lax.all_gather(up_weight, 'sp', axis=0, tiled=True))  142 us
    all_gather x1, waiting for transfers between devices, body(): gate = add_rows(lax.all_gather(gate_weight, 'sp', axis=0, tiled=True))  141 us
    unnamed x68, local copies, waits for them, and re-layouts  21.5 us
  transfers between devices with their start and end apart: 21, of which 20 were waited for; matrix products, arithmetic and copies ran while one was open for 5% of the time, Pallas kernels for 0%

profile of v1, /device:TPU:0, one launch (start us, length us, event | category | flops | bytes accessed | tf_op | source)
XLA Modules:
  0.0 749.6 jit_solution(13346388711540857105)
XLA Ops:
  14.0 8.9 %collective-permute-done = bf16[192,4,128]{2,1,0:T(4,128)(2,1)S(1)} collective-permute-done((bf16[192,4,128]{2,1,0:T(4,128)(2,1)S(1)}, bf16[192,4,128]{2,1,0:T(4,128)(2,1)S(1)}, u32[]{:S(2)}, u32[]{:S(2)}) %collective-permute-start) | collective-permute-done | bytes 196640 | tf_op jit(solution)/shard_map/ppermute | solution.py:93
  22.9 9.7 %collective-permute-done.1 = bf16[192,4,128]{2,1,0:T(4,128)(2,1)S(1)} collective-permute-done((bf16[192,4,128]{2,1,0:T(4,128)(2,1)S(1)}, bf16[192,4,128]{2,1,0:T(4,128)(2,1)S(1)}, u32[]{:S(2)}, u32[]{:S(2)}) %collective-permute-start.1) | collective-permute-done | bytes 196640 | tf_op jit(solution)/shard_map/ppermute | solution.py:93
  32.6 9.3 %collective-permute-done.2 = bf16[192,4,128]{2,1,0:T(4,128)(2,1)S(1)} collective-permute-done((bf16[192,4,128]{2,1,0:T(4,128)(2,1)S(1)}, bf16[192,4,128]{2,1,0:T(4,128)(2,1)S(1)}, u32[]{:S(2)}, u32[]{:S(2)}) %collective-permute-start.2) | collective-permute-done | bytes 196640 | tf_op jit(solution)/shard_map/ppermute | solution.py:93
  41.9 9.3 %collective-permute-done.3 = bf16[192,4,128]{2,1,0:T(4,128)(2,1)S(1)} collective-permute-done((bf16[192,4,128]{2,1,0:T(4,128)(2,1)S(1)}, bf16[192,4,128]{2,1,0:T(4,128)(2,1)S(1)}, u32[]{:S(2)}, u32[]{:S(2)}) %collective-permute-start.3) | collective-permute-done | bytes 196640 | tf_op jit(solution)/shard_map/ppermute | solution.py:93
  51.1 9.3 %collective-permute-done.4 = bf16[192,4,128]{2,1,0:T(4,128)(2,1)S(1)} collective-permute-done((bf16[192,4,128]{2,1,0:T(4,128)(2,1)S(1)}, bf16[192,4,128]{2,1,0:T(4,128)(2,1)S(1)}, u32[]{:S(2)}, u32[]{:S(2)}) %collective-permute-start.4) | collective-permute-done | bytes 196640 | tf_op jit(solution)/shard_map/ppermute | solution.py:93
  60.4 9.3 %collective-permute-done.5 = bf16[192,4,128]{2,1,0:T(4,128)(2,1)S(1)} collective-permute-done((bf16[192,4,128]{2,1,0:T(4,128)(2,1)S(1)}, bf16[192,4,128]{2,1,0:T(4,128)(2,1)S(1)}, u32[]{:S(2)}, u32[]{:S(2)}) %collective-permute-start.5) | collective-permute-done | bytes 196640 | tf_op jit(solution)/shard_map/ppermute | solution.py:93
  69.7 10.4 %collective-permute-done.6 = bf16[192,4,128]{2,1,0:T(4,128)(2,1)S(1)} collective-permute-done((bf16[192,4,128]{2,1,0:T(4,128)(2,1)S(1)}, bf16[192,4,128]{2,1,0:T(4,128)(2,1)S(1)}, u32[]{:S(2)}, u32[]{:S(2)}) %collective-permute-start.6) | collective-permute-done | bytes 196640 | tf_op jit(solution)/shard_map/ppermute | solution.py:93
  80.9 10.3 %collective-permute-done.7 = bf16[192,4,128]{2,1,0:T(4,128)(2,1)S(1)} collective-permute-done((bf16[192,4,128]{2,1,0:T(4,128)(2,1)S(1)}, bf16[192,4,128]{2,1,0:T(4,128)(2,1)S(1)}, u32[]{:S(2)}, u32[]{:S(2)}) %collective-permute-start.7) | collective-permute-done | bytes 196640 | tf_op jit(solution)/shard_map/ppermute | solution.py:93
  91.3 14.1 %collective-permute-done.8 = bf16[192,4,128]{2,1,0:T(4,128)(2,1)S(1)} collective-permute-done((bf16[192,4,128]{2,1,0:T(4,128)(2,1)S(1)}, bf16[192,4,128]{2,1,0:T(4,128)(2,1)S(1)}, u32[]{:S(2)}, u32[]{:S(2)}) %collective-permute-start.8) | collective-permute-done | bytes 196640 | tf_op jit(solution)/shard_map/ppermute | solution.py:93
  105.4 10.2 %collective-permute-done.9 = bf16[192,4,128]{2,1,0:T(4,128)(2,1)S(1)} collective-permute-done((bf16[192,4,128]{2,1,0:T(4,128)(2,1)S(1)}, bf16[192,4,128]{2,1,0:T(4,128)(2,1)S(1)}, u32[]{:S(2)}, u32[]{:S(2)}) %collective-permute-start.9) | collective-permute-done | bytes 196640 | tf_op jit(solution)/shard_map/ppermute | solution.py:93
  115.6 10.2 %collective-permute-done.10 = bf16[192,4,128]{2,1,0:T(4,128)(2,1)S(1)} collective-permute-done((bf16[192,4,128]{2,1,0:T(4,128)(2,1)S(1)}, bf16[192,4,128]{2,1,0:T(4,128)(2,1)S(1)}, u32[]{:S(2)}, u32[]{:S(2)}) %collective-permute-start.10) | collective-permute-done | bytes 196640 | tf_op jit(solution)/shard_map/ppermute | solution.py:93
  126.4 8.7 %collective-permute-done.11 = bf16[192,4,128]{2,1,0:T(4,128)(2,1)S(1)} collective-permute-done((bf16[192,4,128]{2,1,0:T(4,128)(2,1)S(1)}, bf16[192,4,128]{2,1,0:T(4,128)(2,1)S(1)}, u32[]{:S(2)}, u32[]{:S(2)}) %collective-permute-start.11) | collective-permute-done | bytes 196640 | tf_op jit(solution)/shard_map/ppermute | solution.py:93
  135.2 13.5 %collective-permute-done.12 = bf16[192,4,128]{2,1,0:T(4,128)(2,1)S(1)} collective-permute-done((bf16[192,4,128]{2,1,0:T(4,128)(2,1)S(1)}, bf16[192,4,128]{2,1,0:T(4,128)(2,1)S(1)}, u32[]{:S(2)}, u32[]{:S(2)}) %collective-permute-start.12) | collective-permute-done | bytes 196640 | tf_op jit(solution)/shard_map/ppermute | solution.py:93
  149.0 12.9 %collective-permute-done.13 = bf16[192,4,128]{2,1,0:T(4,128)(2,1)} collective-permute-done((bf16[192,4,128]{2,1,0:T(4,128)(2,1)S(1)}, bf16[192,4,128]{2,1,0:T(4,128)(2,1)}, u32[]{:S(2)}, u32[]{:S(2)}) %collective-permute-start.13) | collective-permute-done | bytes 196640 | tf_op jit(solution)/shard_map/ppermute | solution.py:93
  163.8 7.9 %collective-permute-done.14 = bf16[192,4,128]{2,1,0:T(4,128)(2,1)} collective-permute-done((bf16[192,4,128]{2,1,0:T(4,128)(2,1)}, bf16[192,4,128]{2,1,0:T(4,128)(2,1)}, u32[]{:S(2)}, u32[]{:S(2)}) %collective-permute-start.14) | collective-permute-done | bytes 196640 | tf_op jit(solution)/shard_map/ppermute | solution.py:93
  195.9 45.6 %while.15 = (s32[]{:T(128)}, f32[4,2,192]{2,1,0:T(2,128)S(1)}, f32[4,2,192]{2,1,0:T(2,128)S(1)}, f32[4,2,192,128]{3,2,1,0:T(8,128)S(1)}, bf16[4,768,4,128]{3,2,1...) while((s32[]{:T(128)}, f32[4,2,192]{2,1,0:T(2,128)S(1)}, ...), condition=%wide.region_5.6_spmd.clone, body=%wide.region_2.5_spmd.clone.sunk | while | flops 614014464 | bytes 20938860 | solution.py:104
  223.6 3.4 fusion.42
  242.6 4.1 convolution_convert_fusion.1
  254.9 141.3 %all-gather.7.cloned.1.call-done = bf16[2048,2816]{1,0:T(8,128)(2,1)} async-done(((bf16[128,2816]{1,0:T(8,128)(2,1)}), bf16[2048,2816]{1,0:T(8,128)(2,1)}) %all-gather.7.cloned.1.call-update) | async-done | bytes 11534352 | tf_op jit(solution)/shard_map/all_gather | solution.py:126
  396.2 6.7 fusion.24
  402.9 176.1 %all-gather.11.cloned.1.call-done = bf16[2816,2048]{1,0:T(8,128)(2,1)} async-done(((bf16[2816,128]{1,0:T(8,128)(2,1)}), bf16[2816,2048]{1,0:T(8,128)(2,1)}) %all-gather.11.cloned.1.call-update) | async-done | bytes 11534352 | tf_op jit(solution)/shard_map/all_gather | solution.py:129
  579.0 142.2 %all-gather.9.cloned.1.call-done = bf16[2048,2816]{1,0:T(8,128)(2,1)} async-done(((bf16[128,2816]{1,0:T(8,128)(2,1)}), bf16[2048,2816]{1,0:T(8,128)(2,1)}) %all-gather.9.cloned.1.call-update) | async-done | bytes 11534352 | tf_op jit(solution)/shard_map/all_gather | solution.py:127
  721.2 13.2 %convolution_convert_fusion = bf16[192,2048]{1,0:T(8,128)(2,1)} fusion(bf16[2816,2048]{1,0:T(8,128)(2,1)} %all-gather.11.cloned.1.call-done, bf16[192,2048]{1,0:T(8,128)(2,1)S(1)} %all_gather.16, bf16[2048,2816]{1,0:T(8,128)(2,1)} %all-gather.9.cloned.1.call-done, f32[192,2816]{1,0:T(8,128)S(1)} %fusion.24), kind=kOutput, calls=%fused_computation.23 | convolution fusion | flops 4432822272 | bytes 26804224 | tf_op jit(solution)/shard_map/dot_general | solution.py:131
  734.4 6.5 reduce-scatter.5.cloned.1.call-done
  (159 shorter events, 88.2 us)
Async XLA Ops:
  6.5 119.2 %copy-start.13 = (bf16[192,1024]{1,0:T(8,128)(2,1)S(1)}, bf16[192,1024]{1,0:T(8,128)(2,1)}, u32[]{:S(2)}) copy-start(bf16[192,1024]{1,0:T(8,128)(2,1)} %param.14) | copy-start | bytes 1179652
  6.5 142.2 %copy-start.17 = (f32[128]{0:T(128)S(1)}, f32[128]{0:T(128)}, u32[]{:S(2)}) copy-start(f32[128]{0:T(128)} %param.17) | copy-start | bytes 1540
  6.5 189.4 %all-gather.5.cloned.1.call-start = ((), (), s32[]{:S(2)}) async-start(), calls=%async_computation.2 | async-start | bytes 3342336 | tf_op jit(solution)/shard_map/all_gather | solution.py:97
  11.0 11.9 %collective-permute-start = (bf16[192,4,128]{2,1,0:T(4,128)(2,1)S(1)}, bf16[192,4,128]{2,1,0:T(4,128)(2,1)S(1)}, u32[]{:S(2)}, u32[]{:S(2)}) collective-permute-start(bf16[192,4,128]{2,1,0:T(4,128)(2,1)S(1)} %pad_maximum_fusion.1), channel_id=1, source_target_pairs={{0,2},{2,4},{4,6},{6,8},{8,10},{10,12},{12,14},{14,16},{16,18},{18... | collective-permute-start | bytes 589832 | tf_op jit(solution)/shard_map/ppermute | solution.py:93
  22.9 9.7 %collective-permute-start.1 = (bf16[192,4,128]{2,1,0:T(4,128)(2,1)S(1)}, bf16[192,4,128]{2,1,0:T(4,128)(2,1)S(1)}, u32[]{:S(2)}, u32[]{:S(2)}) collective-permute-start(bf16[192,4,128]{2,1,0:T(4,128)(2,1)S(1)} %collective-permute-done), channel_id=1, source_target_pairs={{0,2},{2,4},{4,6},{6,8},{8,10},{10,12},{12,14},{14,16},{16,18},{18... | collective-permute-start | bytes 589832 | tf_op jit(solution)/shard_map/ppermute | solution.py:93
  32.6 9.3 %collective-permute-start.2 = (bf16[192,4,128]{2,1,0:T(4,128)(2,1)S(1)}, bf16[192,4,128]{2,1,0:T(4,128)(2,1)S(1)}, u32[]{:S(2)}, u32[]{:S(2)}) collective-permute-start(bf16[192,4,128]{2,1,0:T(4,128)(2,1)S(1)} %collective-permute-done.1), channel_id=1, source_target_pairs={{0,2},{2,4},{4,6},{6,8},{8,10},{10,12},{12,14},{14,16},{16,18},{18... | collective-permute-start | bytes 589832 | tf_op jit(solution)/shard_map/ppermute | solution.py:93
  41.9 9.3 %collective-permute-start.3 = (bf16[192,4,128]{2,1,0:T(4,128)(2,1)S(1)}, bf16[192,4,128]{2,1,0:T(4,128)(2,1)S(1)}, u32[]{:S(2)}, u32[]{:S(2)}) collective-permute-start(bf16[192,4,128]{2,1,0:T(4,128)(2,1)S(1)} %collective-permute-done.2), channel_id=1, source_target_pairs={{0,2},{2,4},{4,6},{6,8},{8,10},{10,12},{12,14},{14,16},{16,18},{18... | collective-permute-start | bytes 589832 | tf_op jit(solution)/shard_map/ppermute | solution.py:93
  51.1 110.8 %copy-start = (bf16[192,4,128]{2,1,0:T(4,128)(2,1)}, bf16[192,4,128]{2,1,0:T(4,128)(2,1)S(1)}, u32[]{:S(2)}) copy-start(bf16[192,4,128]{2,1,0:T(4,128)(2,1)S(1)} %collective-permute-done.3) | copy-start | bytes 589828
  51.1 9.3 %collective-permute-start.4 = (bf16[192,4,128]{2,1,0:T(4,128)(2,1)S(1)}, bf16[192,4,128]{2,1,0:T(4,128)(2,1)S(1)}, u32[]{:S(2)}, u32[]{:S(2)}) collective-permute-start(bf16[192,4,128]{2,1,0:T(4,128)(2,1)S(1)} %collective-permute-done.3), channel_id=1, source_target_pairs={{0,2},{2,4},{4,6},{6,8},{8,10},{10,12},{12,14},{14,16},{16,18},{18... | collective-permute-start | bytes 589832 | tf_op jit(solution)/shard_map/ppermute | solution.py:93
  60.4 9.3 %collective-permute-start.5 = (bf16[192,4,128]{2,1,0:T(4,128)(2,1)S(1)}, bf16[192,4,128]{2,1,0:T(4,128)(2,1)S(1)}, u32[]{:S(2)}, u32[]{:S(2)}) collective-permute-start(bf16[192,4,128]{2,1,0:T(4,128)(2,1)S(1)} %collective-permute-done.4), channel_id=1, source_target_pairs={{0,2},{2,4},{4,6},{6,8},{8,10},{10,12},{12,14},{14,16},{16,18},{18... | collective-permute-start | bytes 589832 | tf_op jit(solution)/shard_map/ppermute | solution.py:93
  69.7 10.4 %collective-permute-start.6 = (bf16[192,4,128]{2,1,0:T(4,128)(2,1)S(1)}, bf16[192,4,128]{2,1,0:T(4,128)(2,1)S(1)}, u32[]{:S(2)}, u32[]{:S(2)}) collective-permute-start(bf16[192,4,128]{2,1,0:T(4,128)(2,1)S(1)} %collective-permute-done.5), channel_id=1, source_target_pairs={{0,2},{2,4},{4,6},{6,8},{8,10},{10,12},{12,14},{14,16},{16,18},{18... | collective-permute-start | bytes 589832 | tf_op jit(solution)/shard_map/ppermute | solution.py:93
  80.1 11.2 %collective-permute-start.7 = (bf16[192,4,128]{2,1,0:T(4,128)(2,1)S(1)}, bf16[192,4,128]{2,1,0:T(4,128)(2,1)S(1)}, u32[]{:S(2)}, u32[]{:S(2)}) collective-permute-start(bf16[192,4,128]{2,1,0:T(4,128)(2,1)S(1)} %collective-permute-done.6), channel_id=1, source_target_pairs={{0,2},{2,4},{4,6},{6,8},{8,10},{10,12},{12,14},{14,16},{16,18},{18... | collective-permute-start | bytes 589832 | tf_op jit(solution)/shard_map/ppermute | solution.py:93
  80.9 169.9 %reduce-scatter.3.cloned.1.call-start = ((), (), s32[]{:S(2)}) async-start(), calls=%async_computation.3 | async-start | bytes 1179648 | tf_op jit(solution)/shard_map/reduce_scatter | solution.py:113
  91.3 14.1 %collective-permute-start.8 = (bf16[192,4,128]{2,1,0:T(4,128)(2,1)S(1)}, bf16[192,4,128]{2,1,0:T(4,128)(2,1)S(1)}, u32[]{:S(2)}, u32[]{:S(2)}) collective-permute-start(bf16[192,4,128]{2,1,0:T(4,128)(2,1)S(1)} %collective-permute-done.7), channel_id=1, source_target_pairs={{0,2},{2,4},{4,6},{6,8},{8,10},{10,12},{12,14},{14,16},{16,18},{18... | collective-permute-start | bytes 589832 | tf_op jit(solution)/shard_map/ppermute | solution.py:93
  105.4 10.2 %collective-permute-start.9 = (bf16[192,4,128]{2,1,0:T(4,128)(2,1)S(1)}, bf16[192,4,128]{2,1,0:T(4,128)(2,1)S(1)}, u32[]{:S(2)}, u32[]{:S(2)}) collective-permute-start(bf16[192,4,128]{2,1,0:T(4,128)(2,1)S(1)} %collective-permute-done.8), channel_id=1, source_target_pairs={{0,2},{2,4},{4,6},{6,8},{8,10},{10,12},{12,14},{14,16},{16,18},{18... | collective-permute-start | bytes 589832 | tf_op jit(solution)/shard_map/ppermute | solution.py:93
  115.6 10.2 %collective-permute-start.10 = (bf16[192,4,128]{2,1,0:T(4,128)(2,1)S(1)}, bf16[192,4,128]{2,1,0:T(4,128)(2,1)S(1)}, u32[]{:S(2)}, u32[]{:S(2)}) collective-permute-start(bf16[192,4,128]{2,1,0:T(4,128)(2,1)S(1)} %collective-permute-done.9), channel_id=1, source_target_pairs={{0,2},{2,4},{4,6},{6,8},{8,10},{10,12},{12,14},{14,16},{16,18},{18... | collective-permute-start | bytes 589832 | tf_op jit(solution)/shard_map/ppermute | solution.py:93
  125.8 9.3 %collective-permute-start.11 = (bf16[192,4,128]{2,1,0:T(4,128)(2,1)S(1)}, bf16[192,4,128]{2,1,0:T(4,128)(2,1)S(1)}, u32[]{:S(2)}, u32[]{:S(2)}) collective-permute-start(bf16[192,4,128]{2,1,0:T(4,128)(2,1)S(1)} %collective-permute-done.10), channel_id=1, source_target_pairs={{0,2},{2,4},{4,6},{6,8},{8,10},{10,12},{12,14},{14,16},{16,18},{18... | collective-permute-start | bytes 589832 | tf_op jit(solution)/shard_map/ppermute | solution.py:93
  135.1 13.6 %collective-permute-start.12 = (bf16[192,4,128]{2,1,0:T(4,128)(2,1)S(1)}, bf16[192,4,128]{2,1,0:T(4,128)(2,1)S(1)}, u32[]{:S(2)}, u32[]{:S(2)}) collective-permute-start(bf16[192,4,128]{2,1,0:T(4,128)(2,1)S(1)} %collective-permute-done.11), channel_id=1, source_target_pairs={{0,2},{2,4},{4,6},{6,8},{8,10},{10,12},{12,14},{14,16},{16,18},{18... | collective-permute-start | bytes 589832 | tf_op jit(solution)/shard_map/ppermute | solution.py:93
  148.7 13.2 %collective-permute-start.13 = (bf16[192,4,128]{2,1,0:T(4,128)(2,1)S(1)}, bf16[192,4,128]{2,1,0:T(4,128)(2,1)}, u32[]{:S(2)}, u32[]{:S(2)}) collective-permute-start(bf16[192,4,128]{2,1,0:T(4,128)(2,1)S(1)} %collective-permute-done.12), channel_id=1, source_target_pairs={{0,2},{2,4},{4,6},{6,8},{8,10},{10,12},{12,14},{14,16},{16,18},{18... | collective-permute-start | bytes 589832 | tf_op jit(solution)/shard_map/ppermute | solution.py:93
  161.9 9.8 %collective-permute-start.14 = (bf16[192,4,128]{2,1,0:T(4,128)(2,1)}, bf16[192,4,128]{2,1,0:T(4,128)(2,1)}, u32[]{:S(2)}, u32[]{:S(2)}) collective-permute-start(bf16[192,4,128]{2,1,0:T(4,128)(2,1)} %collective-permute-done.13), channel_id=1, source_target_pairs={{0,2},{2,4},{4,6},{6,8},{8,10},{10,12},{12,14},{14,16},{16,18},{18... | collective-permute-start | bytes 589832 | tf_op jit(solution)/shard_map/ppermute | solution.py:93
  246.7 149.5 %all-gather.7.cloned.1.call-start = ((), (), s32[]{:S(2)}) async-start(), calls=%async_computation.4 | async-start | bytes 12255232 | tf_op jit(solution)/shard_map/all_gather | solution.py:126
  247.4 331.6 %all-gather.11.cloned.1.call-start = ((), (), s32[]{:S(2)}) async-start(), calls=%async_computation.6 | async-start | bytes 12255232 | tf_op jit(solution)/shard_map/all_gather | solution.py:129
  248.0 473.3 %all-gather.9.cloned.1.call-start = ((), (), s32[]{:S(2)}) async-start(), calls=%async_computation.5 | async-start | bytes 12255232 | tf_op jit(solution)/shard_map/all_gather | solution.py:127
  248.6 492.4 %reduce-scatter.5.cloned.1.call-start = ((), (), s32[]{:S(2)}) async-start(), calls=%async_computation.7 | async-start | bytes 1179648 | tf_op jit(solution)/shard_map/reduce_scatter | solution.py:130
  (15 other events, 584.3 us)
Sparse Core Ops, SparseCore 0:
  81.0 76.5 all-gather.4
  246.8 4.0 reduce-scatter.2
  253.6 142.5 all-gather.6
  398.7 180.2 all-gather.10
  581.6 139.5 all-gather.8
  734.5 6.3 reduce-scatter.4
